TPU v7x, 32 devices: a whole 2x2x4 slice. The times are simulated.
32 devices in a mesh: fs: 4 (over y, x), tp: 8 (over z, core).
Axes of the slice: x: 2, y: 2, z: 4, core: 2. Of those that a mesh axis runs over, the one named last changes fastest.
Arguments:
- tokens: bfloat16 [4096, 2048], P(('fs', 'tp')), may hold values from -6 to 6
- norm_gain: float32 [2048], replicated, may hold values from 0.1 to 1.9
- gate_weight: bfloat16 [2048, 5632], P('fs', 'tp'), may hold values from -0.125 to 0.125
- up_weight: bfloat16 [2048, 5632], P('fs', 'tp'), may hold values from -0.125 to 0.125
- down_weight: bfloat16 [5632, 2048], P('tp', 'fs'), may hold values from -0.078125 to 0.078125
Outputs:
- mixed: bfloat16 [4096, 2048], P(('fs', 'tp'))
All inputs are finite; a program needn't handle non-finite values.
Results may differ from a plain program's by a relative error of at most 0.0065.
Values may be sent and summed in bfloat16 or wider, within the bound.
A program may use at most 128 MiB of HBM per device.

v0:
```python
import jax
import jax.numpy as jnp
from jax import lax
from jax.sharding import PartitionSpec as P

eps_floor = 0.05


def local(tokens, norm_gain, gate_weight, up_weight, down_weight):
    values = tokens.astype(jnp.float32)
    factor = lax.rsqrt(jnp.mean(values * values, axis=-1, keepdims=True) + eps_floor)
    normed = (values * factor * norm_gain).astype(jnp.bfloat16)
    local_ff = gate_weight.shape[1]
    group = lax.all_gather(normed, "tp", axis=0, tiled=True)
    joined = jnp.concatenate(
        (
            lax.all_gather(gate_weight, "fs", axis=0, tiled=True),
            lax.all_gather(up_weight, "fs", axis=0, tiled=True),
        ),
        axis=1,
    )
    product = jnp.dot(group, joined, preferred_element_type=jnp.float32)
    hidden = (jax.nn.silu(product[:, :local_ff]) * product[:, local_ff:]).astype(jnp.bfloat16)
    down_local = lax.all_gather(down_weight, "fs", axis=1, tiled=True)
    mixed = lax.psum_scatter(
        jnp.dot(hidden, down_local, preferred_element_type=jnp.float32),
        "tp",
        scatter_dimension=0,
        tiled=True,
    )
    return mixed.astype(jnp.bfloat16)


def solution(mesh):
    return jax.shard_map(
        local,
        mesh=mesh,
        in_specs=(P(("fs", "tp"), None), P(), P("fs", "tp"), P("fs", "tp"), P("tp", "fs")),
        out_specs=P(("fs", "tp"), None),
        check_vma=False,
    )
```

profile of v0, /device:TPU:0, one launch (start us, length us, event | category | flops | bytes accessed | tf_op | source)
XLA Modules:
  0.0 296.1 jit_solution(4076748041551358290)
XLA Ops:
  6.5 0.0 all-gather.7.cloned.1.call-start
  6.5 0.7 all-gather.7.cloned.1.call-update
  7.3 0.0 all-gather.9.cloned.1.call-start
  7.3 0.7 all-gather.9.cloned.1.call-update
  8.0 0.0 all-gather.5.cloned.1.call-start
  8.1 1.2 fusion.8
  9.3 2.0 fusion.10
  11.3 0.0 all-gather.5.cloned.1.call-update
  11.3 0.0 all-gather.11.cloned.1.call-start
  11.4 0.5 all-gather.11.cloned.1.call-update
  11.9 0.0 reduce-scatter.2.cloned.1.call-start
  12.0 41.5 %all-gather.7.cloned.1.call-done = bf16[2048,704]{0,1:T(8,128)(2,1)} async-done(((bf16[512,704]{0,1:T(8,128)(2,1)}), bf16[2048,704]{0,1:T(8,128)(2,1)}) %all-gather.7.cloned.1.call-update) | async-done | bytes 2883600 | tf_op jit(solution)/shard_map/all_gather | solution.py:17
  53.5 43.4 %all-gather.9.cloned.1.call-done = bf16[2048,704]{0,1:T(8,128)(2,1)} async-done(((bf16[512,704]{0,1:T(8,128)(2,1)}), bf16[2048,704]{0,1:T(8,128)(2,1)}) %all-gather.9.cloned.1.call-update) | async-done | bytes 2883600 | tf_op jit(solution)/shard_map/all_gather | solution.py:18
  96.9 48.5 %all-gather.5.cloned.1.call-done = bf16[1024,2048]{1,0:T(8,128)(2,1)} async-done(((bf16[128,2048]{1,0:T(8,128)(2,1)}), bf16[1024,2048]{1,0:T(8,128)(2,1)}) %all-gather.5.cloned.1.call-update) | async-done | bytes 4194320 | tf_op jit(solution)/shard_map/all_gather | solution.py:14
  145.4 11.8 %fusion = f32[1024,1408]{1,0:T(8,128)} fusion(bf16[1024,2048]{1,0:T(8,128)(2,1)} %all-gather.5.cloned.1.call-done, bf16[2048,704]{0,1:T(8,128)(2,1)} %all-gather.9.cloned.1.call-done, bf16[2048,704]{0,1:T(8,128)(2,1)} %all-gather.7.cloned.1.call-done), kind=kOutput, calls=%fused_computation | convolution fusion | flops 5917114368 | bytes 15728640 | tf_op jit(solution)/shard_map/dot_general | solution.py:22
  157.2 30.2 %all-gather.11.cloned.1.call-done = bf16[704,2048]{1,0:T(8,128)(2,1)} async-done(((bf16[704,512]{1,0:T(8,128)(2,1)}), bf16[704,2048]{1,0:T(8,128)(2,1)}) %all-gather.11.cloned.1.call-update) | async-done | bytes 2883600 | tf_op jit(solution)/shard_map/all_gather | solution.py:24
  187.4 10.4 %fusion.5 = f32[1024,2048]{1,0:T(8,128)} fusion(bf16[704,2048]{1,0:T(8,128)(2,1)} %all-gather.11.cloned.1.call-done, f32[1024,1408]{1,0:T(8,128)} %fusion), kind=kOutput, calls=%fused_computation.6 | convolution fusion | flops 2957115392 | bytes 17563648 | tf_op jit(solution)/shard_map/dot_general | solution.py:26
  197.8 0.0 reduce-scatter.2.cloned.1.call-update
  197.8 89.7 %reduce-scatter.2.cloned.1.call-done = f32[128,2048]{1,0:T(8,128)} async-done(((f32[1024,2048]{1,0:T(8,128)}), f32[128,2048]{1,0:T(8,128)}) %reduce-scatter.2.cloned.1.call-update) | async-done | bytes 1048592 | tf_op jit(solution)/shard_map/reduce_scatter | solution.py:25
  287.5 2.1 convert_element_type.15
  (1 shorter events, 0.0 us)
Async XLA Ops:
  6.5 46.9 %all-gather.7.cloned.1.call-start = ((), (), s32[]{:S(2)}) async-start(), calls=%async_computation.2 | async-start | bytes 3604480 | tf_op jit(solution)/shard_map/all_gather | solution.py:17
  7.3 89.6 %all-gather.9.cloned.1.call-start = ((), (), s32[]{:S(2)}) async-start(), calls=%async_computation.3 | async-start | bytes 3604480 | tf_op jit(solution)/shard_map/all_gather | solution.py:18
  8.0 137.3 %all-gather.5.cloned.1.call-start = ((), (), s32[]{:S(2)}) async-start(), calls=%async_computation.1 | async-start | bytes 4718592 | tf_op jit(solution)/shard_map/all_gather | solution.py:14
  11.3 176.1 %all-gather.11.cloned.1.call-start = ((), (), s32[]{:S(2)}) async-start(), calls=%async_computation.4 | async-start | bytes 3604480 | tf_op jit(solution)/shard_map/all_gather | solution.py:24
  11.9 275.6 %reduce-scatter.2.cloned.1.call-start = ((), (), s32[]{:S(2)}) async-start(), calls=%async_computation.5 | async-start | bytes 9437184 | tf_op jit(solution)/shard_map/reduce_scatter | solution.py:25
Sparse Core Ops, SparseCore 0:
  9.2 44.2 all-gather.6
  55.3 41.5 all-gather.8
  98.5 46.8 all-gather.4
  147.0 40.3 all-gather.10
  198.0 89.5 reduce-scatter.1
where the time goes:
time: 296 us
  waiting for transfers between devices  255 us (86%)
  matrix products  22.2 us (8%)
  between operations  13.1 us (4%)
  other arithmetic  5.35 us (2%)
    reduce_scatter x1, waiting for transfers between devices, local(): lax.psum_scatter(jnp.dot(hidden, down_local, preferred_element_type=jnp.f...  89.7 us
    all_gather x1, waiting for transfers between devices, local(): group = lax.all_gather(normed, 'tp', axis=0, tiled=True)  48.5 us
    all_gather x1, waiting for transfers between devices, local(): lax.all_gather(up_weight, 'fs', axis=0, tiled=True)  43.4 us
    all_gather x1, waiting for transfers between devices, local(): lax.all_gather(gate_weight, 'fs', axis=0, tiled=True)  41.5 us
    all_gather x1, waiting for transfers between devices, local(): down_local = lax.all_gather(down_weight, 'fs', axis=1, tiled=True)  30.2 us
    dot_general x1, matrix products, local(): product = jnp.dot(group, joined, preferred_element_type=jnp.float32)  11.8 us
    dot_general x1, matrix products, local(): jnp.dot(hidden, down_local, preferred_element_type=jnp.float32)  10.4 us
  transfers between devices with their start and end apart: 5, of which 5 were waited for; matrix products, arithmetic and copies ran while one was open for 5% of the time, Pallas kernels for 0%

commit v1 on v0

--- a/solution.py
+++ b/solution.py
@@ -21,7 +21,12 @@
     )
     product = jnp.dot(group, joined, preferred_element_type=jnp.float32)
     hidden = (jax.nn.silu(product[:, :local_ff]) * product[:, local_ff:]).astype(jnp.bfloat16)
-    down_local = lax.all_gather(down_weight, "fs", axis=1, tiled=True)
+    ring = [down_weight]
+    for hop in range(3):
+        ring.append(lax.ppermute(ring[-1], "fs", [(dev, (dev + 1) % 4) for dev in range(4)]))
+    down_local = jnp.roll(
+        jnp.concatenate(ring[::-1], axis=1), (lax.axis_index("fs") + 1) * ring[0].shape[1], axis=1
+    )
     mixed = lax.psum_scatter(
         jnp.dot(hidden, down_local, preferred_element_type=jnp.float32),
         "tp",

time: 296 us -> 284 us (0.959)
  waiting for transfers between devices: 255 us -> 234 us
  local copies, waits for them, and re-layouts: 0 us -> 8.03 us
  starting transfers between devices: 0.16 us -> 4.87 us
  matrix products: 22.2 us -> 18.4 us
    ppermute x0 -> x3, waiting for transfers between devices: none -> 73.6 us  [local(): lax.ppermute(ring[-1], 'fs', [(dev, (dev + 1) % 4) for dev in range(4)])]
    all_gather x1, waiting for transfers between devices: 41.5 us -> 0.01 us  [local(): lax.all_gather(gate_weight, 'fs', axis=0, tiled=True)]
    all_gather x1 -> x0, waiting for transfers between devices: 30.2 us -> none  [local(): down_local = lax.all_gather(down_weight, 'fs', axis=1, tiled=True)]
    all_gather x1, waiting for transfers between devices: 43.4 us -> 21.9 us  [local(): lax.all_gather(up_weight, 'fs', axis=0, tiled=True)]
    unnamed x0 -> x9, local copies, waits for them, and re-layouts: none -> 7.05 us
    ppermute x0 -> x3, starting transfers between devices: none -> 4.75 us  [local(): lax.ppermute(ring[-1], 'fs', [(dev, (dev + 1) % 4) for dev in range(4)])]
  transfers between devices with their start and end apart: 5 -> 7, of which waited for: 5 -> 6; matrix products, arithmetic and copies ran while one was open for 5% -> 4% of each run, Pallas kernels for 0% -> 0%
where the time goes in v1:
time: 284 us
  waiting for transfers between devices  234 us (82%)
  matrix products  18.4 us (6%)
  between operations  13.1 us (5%)
  local copies, waits for them, and re-layouts  8.03 us (3%)
  other arithmetic  5.35 us (2%)
  starting transfers between devices  4.87 us (2%)
    reduce_scatter x1, waiting for transfers between devices, local(): lax.psum_scatter(jnp.dot(hidden, down_local, preferred_element_type=jnp.f...  88.5 us
    ppermute x3, waiting for transfers between devices, local(): lax.ppermute(ring[-1], 'fs', [(dev, (dev + 1) % 4) for dev in range(4)])  73.6 us
    all_gather x1, waiting for transfers between devices, local(): group = lax.all_gather(normed, 'tp', axis=0, tiled=True)  48.5 us
    all_gather x1, waiting for transfers between devices, local(): lax.all_gather(up_weight, 'fs', axis=0, tiled=True)  21.9 us
    dot_general x1, matrix products, local(): product = jnp.dot(group, joined, preferred_element_type=jnp.float32)  10.8 us
    dot_general x1, matrix products, local(): jnp.dot(hidden, down_local, preferred_element_type=jnp.float32)  7.69 us
    unnamed x9, local copies, waits for them, and re-layouts  7.05 us
  transfers between devices with their start and end apart: 7, of which 6 were waited for; matrix products, arithmetic and copies ran while one was open for 4% of the time, Pallas kernels for 0%

profile of v1, /device:TPU:0, one launch (start us, length us, event | category | flops | bytes accessed | tf_op | source)
XLA Modules:
  0.0 283.8 jit_solution(17503648726439948337)
XLA Ops:
  6.5 0.0 copy-start
  6.5 0.0 all-gather.6.cloned.1.call-start
  6.5 0.7 all-gather.6.cloned.1.call-update
  7.3 0.0 all-gather.8.cloned.1.call-start
  7.3 0.7 all-gather.8.cloned.1.call-update
  8.0 0.0 all-gather.4.cloned.1.call-start
  8.1 1.2 fusion.9
  9.3 2.0 fusion.11
  11.3 0.0 all-gather.4.cloned.1.call-update
  11.3 0.0 reduce-scatter.2.cloned.1.call-start
  11.4 3.0 %collective-permute-start = (bf16[704,512]{1,0:T(8,128)(2,1)}, bf16[704,512]{1,0:T(8,128)(2,1)S(1)}, u32[]{:S(2)}, u32[]{:S(2)}) collective-permute-start(bf16[704,512]{1,0:T(8,128)(2,1)} %param.9), channel_id=1, source_target_pairs={{0,8},{8,16},{16,24},{24,0},{1,9},{9,17},{17,25},{25,1},{2,10},{10... | collective-permute-start | bytes 2162696 | tf_op jit(solution)/shard_map/ppermute | solution.py:26
  14.4 25.0 %collective-permute-done = bf16[704,512]{1,0:T(8,128)(2,1)S(1)} collective-permute-done((bf16[704,512]{1,0:T(8,128)(2,1)}, bf16[704,512]{1,0:T(8,128)(2,1)S(1)}, u32[]{:S(2)}, u32[]{:S(2)}) %collective-permute-start) | collective-permute-done | bytes 720928 | tf_op jit(solution)/shard_map/ppermute | solution.py:26
  39.4 0.8 collective-permute-start.1
  40.2 31.1 %collective-permute-done.1 = bf16[704,512]{1,0:T(8,128)(2,1)S(1)} collective-permute-done((bf16[704,512]{1,0:T(8,128)(2,1)S(1)}, bf16[704,512]{1,0:T(8,128)(2,1)S(1)}, u32[]{:S(2)}, u32[]{:S(2)}) %collective-permute-start.1) | collective-permute-done | bytes 720928 | tf_op jit(solution)/shard_map/ppermute | solution.py:26
  71.3 0.9 collective-permute-start.2
  72.2 17.5 %collective-permute-done.2 = bf16[704,512]{1,0:T(8,128)(2,1)S(1)} collective-permute-done((bf16[704,512]{1,0:T(8,128)(2,1)S(1)}, bf16[704,512]{1,0:T(8,128)(2,1)S(1)}, u32[]{:S(2)}, u32[]{:S(2)}) %collective-permute-start.2) | collective-permute-done | bytes 720928 | tf_op jit(solution)/shard_map/ppermute | solution.py:26
  89.8 1.0 constant_dynamic-update-slice_fusion.7
  90.8 1.0 constant_dynamic-update-slice_fusion.6
  91.8 1.0 constant_dynamic-update-slice_fusion.5
  92.7 0.0 copy-done
  92.7 1.0 constant_dynamic-update-slice_fusion.4
  93.8 1.0 constant_dynamic-update-slice_fusion.3
  94.8 1.1 constant_dynamic-update-slice_fusion.2
  95.9 1.0 constant_dynamic-update-slice_fusion.1
  96.9 1.0 constant_dynamic-update-slice_fusion
  97.8 21.9 %all-gather.8.cloned.1.call-done = bf16[2048,704]{0,1:T(8,128)(2,1)} async-done(((bf16[512,704]{0,1:T(8,128)(2,1)}), bf16[2048,704]{0,1:T(8,128)(2,1)}) %all-gather.8.cloned.1.call-update) | async-done | bytes 2883600 | tf_op jit(solution)/shard_map/all_gather | solution.py:18
  119.7 48.5 %all-gather.4.cloned.1.call-done = bf16[1024,2048]{1,0:T(8,128)(2,1)} async-done(((bf16[128,2048]{1,0:T(8,128)(2,1)}), bf16[1024,2048]{1,0:T(8,128)(2,1)}) %all-gather.4.cloned.1.call-update) | async-done | bytes 4194320 | tf_op jit(solution)/shard_map/all_gather | solution.py:14
  168.2 10.8 %fusion = f32[1024,1408]{1,0:T(8,128)S(1)} fusion(bf16[1024,2048]{1,0:T(8,128)(2,1)} %all-gather.4.cloned.1.call-done, bf16[2048,704]{0,1:T(8,128)(2,1)} %all-gather.8.cloned.1.call-done, bf16[2048,704]{0,1:T(8,128)(2,1)} %all-gather.6.cloned.1.call-done), kind=kOutput, calls=%fused_computation | convolution fusion | flops 5917114368 | bytes 15728640 | tf_op jit(solution)/shard_map/dot_general | solution.py:22
  179.0 7.7 %fusion.5 = f32[1024,2048]{1,0:T(8,128)} fusion(bf16[704,4096]{1,0:T(8,128)(2,1)} %constant_dynamic-update-slice_fusion, s32[]{:T(128)S(6)} %select_n.14, f32[1024,1408]{1,0:T(8,128)S(1)} %fusion), kind=kOutput, calls=%fused_computation.6 | convolution fusion | flops 2957115392 | bytes 17563652 | tf_op jit(solution)/shard_map/dot_general | solution.py:31
  186.7 0.0 reduce-scatter.2.cloned.1.call-update
  186.7 88.5 %reduce-scatter.2.cloned.1.call-done = f32[128,2048]{1,0:T(8,128)} async-done(((f32[1024,2048]{1,0:T(8,128)}), f32[128,2048]{1,0:T(8,128)}) %reduce-scatter.2.cloned.1.call-update) | async-done | bytes 1048592 | tf_op jit(solution)/shard_map/reduce_scatter | solution.py:30
  275.2 2.1 convert_element_type.15
  (2 shorter events, 0.0 us)
Async XLA Ops:
  6.5 86.2 %copy-start = (bf16[704,512]{1,0:T(8,128)(2,1)S(1)}, bf16[704,512]{1,0:T(8,128)(2,1)}, u32[]{:S(2)}) copy-start(bf16[704,512]{1,0:T(8,128)(2,1)} %param.9) | copy-start | bytes 2162692
  6.5 91.3 %all-gather.6.cloned.1.call-start = ((), (), s32[]{:S(2)}) async-start(), calls=%async_computation.2 | async-start | bytes 3604480 | tf_op jit(solution)/shard_map/all_gather | solution.py:17
  7.3 112.4 %all-gather.8.cloned.1.call-start = ((), (), s32[]{:S(2)}) async-start(), calls=%async_computation.3 | async-start | bytes 3604480 | tf_op jit(solution)/shard_map/all_gather | solution.py:18
  8.0 160.2 %all-gather.4.cloned.1.call-start = ((), (), s32[]{:S(2)}) async-start(), calls=%async_computation.1 | async-start | bytes 4718592 | tf_op jit(solution)/shard_map/all_gather | solution.py:14
  11.3 263.8 %reduce-scatter.2.cloned.1.call-start = ((), (), s32[]{:S(2)}) async-start(), calls=%async_computation.4 | async-start | bytes 9437184 | tf_op jit(solution)/shard_map/reduce_scatter | solution.py:30
  11.4 28.0 %collective-permute-start = (bf16[704,512]{1,0:T(8,128)(2,1)}, bf16[704,512]{1,0:T(8,128)(2,1)S(1)}, u32[]{:S(2)}, u32[]{:S(2)}) collective-permute-start(bf16[704,512]{1,0:T(8,128)(2,1)} %param.9), channel_id=1, source_target_pairs={{0,8},{8,16},{16,24},{24,0},{1,9},{9,17},{17,25},{25,1},{2,10},{10... | collective-permute-start | bytes 2162696 | tf_op jit(solution)/shard_map/ppermute | solution.py:26
  39.4 31.9 %collective-permute-start.1 = (bf16[704,512]{1,0:T(8,128)(2,1)S(1)}, bf16[704,512]{1,0:T(8,128)(2,1)S(1)}, u32[]{:S(2)}, u32[]{:S(2)}) collective-permute-start(bf16[704,512]{1,0:T(8,128)(2,1)S(1)} %collective-permute-done), channel_id=1, source_target_pairs={{0,8},{8,16},{16,24},{24,0},{1,9},{9,17},{17,25},{25,1},{2,10},{10... | collective-permute-start | bytes 2162696 | tf_op jit(solution)/shard_map/ppermute | solution.py:26
  71.3 18.5 %collective-permute-start.2 = (bf16[704,512]{1,0:T(8,128)(2,1)S(1)}, bf16[704,512]{1,0:T(8,128)(2,1)S(1)}, u32[]{:S(2)}, u32[]{:S(2)}) collective-permute-start(bf16[704,512]{1,0:T(8,128)(2,1)S(1)} %collective-permute-done.1), channel_id=1, source_target_pairs={{0,8},{8,16},{16,24},{24,0},{1,9},{9,17},{17,25},{25,1},{2,10},{10... | collective-permute-start | bytes 2162696 | tf_op jit(solution)/shard_map/ppermute | solution.py:26
Sparse Core Ops, SparseCore 0:
  9.2 65.8 all-gather.5
  76.8 42.8 all-gather.7
  121.3 46.8 all-gather.3
  186.8 88.3 reduce-scatter.1
